TPU v7x, 32 devices: a whole 2x2x4 slice. The times are simulated.
32 devices in a mesh: ep: 8 (over z, core), tp: 4 (over y, x).
Axes of the slice: x: 2, y: 2, z: 4, core: 2. Of those that a mesh axis runs over, the one named last changes fastest.
Arguments:
- mixer_input: bfloat16 [2048, 2048], P('ep'), may hold values from -6 to 6
- mixer_gain: float32 [2048], replicated, may hold values from 0.1 to 1.9
- query_weight: bfloat16 [2048, 2048], P(None, 'tp'), may hold values from -0.13258252 to 0.13258252
- key_weight: bfloat16 [2048, 1024], P(None, 'tp'), may hold values from -2.78423295 to 2.78423295
- value_weight: bfloat16 [2048, 1024], P(None, 'tp'), may hold values from -0.125 to 0.125
- output_weight: bfloat16 [2048, 2048], P(None, 'tp'), may hold values from -1 to 1
- sink_logit: float32 [32], P('tp'), may hold values from 2 to 7
- expert_input: bfloat16 [1024, 2048], P('ep'), may hold values from -6 to 6
- expert_gain: float32 [2048], replicated, may hold values from 0.1 to 1.9
- routes: int32 [1024, 4], P('ep'), may hold values from 0 to 7, all different within a row; in each aligned block of 128 rows (0 to 127, 128 to 255, ...) at most 128 rows name the same one
- route_logits: float32 [1024, 4], P('ep'), may hold values from -6 to 6
- gate_weight: bfloat16 [8, 2048, 2048], P('ep', None, 'tp'), may hold values from -0.375 to 0.375
- up_weight: bfloat16 [8, 2048, 2048], P('ep', None, 'tp'), may hold values from -0.375 to 0.375
- down_weight: bfloat16 [8, 2048, 2048], P('ep', None, 'tp'), may hold values from -0.03125 to 0.03125
Outputs:
- mixer_output: bfloat16 [2048, 2048], P('ep', 'tp')
- expert_output: bfloat16 [1024, 2048], P('ep', 'tp')
Inputs may be any that keep to these rules, and one draw needn't show every extreme that they name: `routes`: each token names 4 different experts. Among the 128 tokens of one index of ep (aligned blocks) no expert is named more than 128 times, and in some blocks one expert is named exactly 128 times.
All inputs are finite; a program needn't handle non-finite values.
Results may differ from a plain program's by a relative error of at most 0.0055.
The roundings to bfloat16 on the way count: a program that leaves them out, or rounds other values in their place, can miss the bound.
Values may be sent and summed in bfloat16 or wider, within the bound.
A program may use at most 64 MiB of HBM per device.

v0:
```python
import jax
import jax.numpy as jnp
from jax import lax
from jax.sharding import PartitionSpec as P

HEAD_DIM = 64
TOP_K = 4
WINDOW = 128
GRID_W = 64
EPSILON = 1e-06
LIMIT = 7.0
SLOPE = 1.702
BASE = 10000.0


def extended(shard, sides, width):
    for axis, dim in sides:
        devices, length = (lax.axis_size(axis), shard.shape[dim])
        up = [(i, (i + 1) % devices) for i in range(devices - 1)]
        down = [(j, i) for i, j in up]
        last = lax.slice_in_dim(shard, length - width, length, axis=dim)
        first = lax.slice_in_dim(shard, 0, width, axis=dim)
        before = lax.ppermute(last, axis, up)
        after = lax.ppermute(first, axis, down)
        shard = jnp.concatenate([before, shard, after], axis=dim)
    return shard


def normalize(rows, gain):
    values = rows.astype(jnp.float32)
    scaled = values * lax.rsqrt(jnp.mean(values * values, axis=-1, keepdims=True) + EPSILON)
    return (scaled * gain).astype(jnp.bfloat16)


def turn(values, cosine, sine):
    first, second = jnp.split(values, 2, axis=-1)
    cosine = cosine[:, None, :]
    sine = sine[:, None, :]
    return jnp.concatenate(
        [first * cosine - second * sine, second * cosine + first * sine], axis=-1
    )


def axial_rope(values, places):
    quarter = values.shape[-1] // 4
    frequency = BASE ** (-jnp.arange(quarter, dtype=jnp.float32) / quarter)
    row_angle = (places // GRID_W).astype(jnp.float32)[:, None] * frequency[None, :]
    column_angle = (places % GRID_W).astype(jnp.float32)[:, None] * frequency[None, :]
    row_part, column_part = jnp.split(values, 2, axis=-1)
    return jnp.concatenate(
        [
            turn(row_part, jnp.cos(row_angle), jnp.sin(row_angle)),
            turn(column_part, jnp.cos(column_angle), jnp.sin(column_angle)),
        ],
        axis=-1,
    )


def activate(gate, up):
    capped = jnp.minimum(gate, LIMIT)
    bounded = jnp.clip(up, -LIMIT, LIMIT)
    return (capped * jax.nn.sigmoid(SLOPE * capped) * (bounded + 1.0)).astype(jnp.bfloat16)


def add_product(piece, weight):
    return jnp.dot(piece, weight, preferred_element_type=jnp.float32)


def shards(
    mixer_input,
    mixer_gain,
    query_weight,
    key_weight,
    value_weight,
    output_weight,
    sink_logit,
    expert_input,
    expert_gain,
    routes,
    route_logits,
    gate_weight,
    up_weight,
    down_weight,
):
    tokens = mixer_input.shape[0]
    query_heads = query_weight.shape[1] // HEAD_DIM
    key_heads = key_weight.shape[1] // HEAD_DIM
    group = query_heads // key_heads
    blocks = tokens // WINDOW
    offset = lax.axis_index("ep") * tokens
    length = lax.axis_size("ep") * tokens
    places = offset + jnp.arange(tokens, dtype=jnp.int32)
    normed = normalize(mixer_input, mixer_gain)
    query = jnp.dot(normed, query_weight, preferred_element_type=jnp.float32).reshape(
        tokens, query_heads, HEAD_DIM
    )
    query = (
        axial_rope(query, places)
        .astype(jnp.bfloat16)
        .reshape(blocks, WINDOW, key_heads, group, HEAD_DIM)
    )
    keys = jnp.dot(normed, key_weight, preferred_element_type=jnp.float32).reshape(
        tokens, key_heads, HEAD_DIM
    )
    keys = axial_rope(keys, places).astype(jnp.bfloat16).reshape(tokens, key_heads * HEAD_DIM)
    values = jnp.dot(normed, value_weight, preferred_element_type=jnp.float32).astype(jnp.bfloat16)
    stacked = jnp.concatenate([keys, values], axis=1)
    widened = extended(stacked, (("ep", 0),), WINDOW)
    framed = widened.reshape(blocks + 2, WINDOW, 2, key_heads, HEAD_DIM)
    nearby = jnp.concatenate([framed[:-2], framed[1:-1], framed[2:]], axis=1)
    scores = jnp.einsum(
        "nqgrd,nkgd->ngrqk", query, nearby[:, :, 0], preferred_element_type=jnp.float32
    ) * HEAD_DIM ** (-0.5)
    query_place = places.reshape(blocks, WINDOW)
    key_place = (
        offset
        + (jnp.arange(blocks, dtype=jnp.int32)[:, None] - 1) * WINDOW
        + jnp.arange(3 * WINDOW, dtype=jnp.int32)[None, :]
    )
    allowed = (
        (jnp.abs(query_place[:, :, None] - key_place[:, None, :]) <= WINDOW)
        & (key_place[:, None, :] >= 0)
        & (key_place[:, None, :] < length)
    )
    scores = jnp.where(allowed[:, None, None], scores, -1e30)
    sinks = sink_logit.reshape(key_heads, group)[None, :, :, None]
    top = jnp.maximum(jnp.max(scores, axis=-1), sinks)
    weights = jnp.exp(scores - top[..., None])
    denominator = jnp.sum(weights, axis=-1) + jnp.exp(sinks - top)
    shares = (weights / denominator[..., None]).astype(jnp.bfloat16)
    mixed = jnp.einsum(
        "ngrqk,nkgd->nqgrd", shares, nearby[:, :, 1], preferred_element_type=jnp.float32
    )
    mixed = mixed.astype(jnp.bfloat16).reshape(tokens, query_heads * HEAD_DIM)
    experts = lax.axis_size("ep")
    rows_here = expert_input.shape[0]
    capacity = 2 * rows_here * TOP_K // experts
    expert_normed = normalize(expert_input, expert_gain)
    chances = jax.nn.softmax(route_logits, axis=-1)
    chosen = routes.reshape(-1)
    marks = (chosen[:, None] == jnp.arange(experts, dtype=jnp.int32)[None, :]).astype(jnp.int32)
    earlier = jnp.sum((jnp.cumsum(marks, axis=0) - marks) * marks, axis=1)
    target = chosen * capacity + earlier
    source = (
        jnp.full((experts * capacity,), rows_here, jnp.int32)
        .at[target]
        .set(jnp.arange(chosen.shape[0], dtype=jnp.int32) // TOP_K)
    )
    padded = jnp.concatenate(
        [expert_normed, jnp.zeros((1, expert_normed.shape[1]), jnp.bfloat16)], axis=0
    )
    down_local = down_weight[0]
    gate_local = gate_weight[0]
    up_local = up_weight[0]
    width = padded.shape[1] // lax.axis_size("tp")
    own = lax.dynamic_slice_in_dim(padded, lax.axis_index("tp") * width, width, 1)
    outgoing = own[source].reshape(experts, capacity, width)
    received = lax.all_to_all(outgoing, "ep", split_axis=0, concat_axis=0, tiled=True)
    flat = received.reshape(experts * capacity, width)
    head_piece = lax.all_gather(mixed, "tp", axis=1, tiled=True)
    feature_piece = lax.all_gather(flat, "tp", axis=1, tiled=True)
    mixer_total = add_product(head_piece, output_weight)
    gate = add_product(feature_piece, gate_local)
    up = add_product(feature_piece, up_local)
    hidden = activate(gate, up)
    result = add_product(lax.all_gather(hidden, "tp", axis=1, tiled=True), down_local)
    result = result.astype(jnp.bfloat16).reshape(experts, capacity, down_local.shape[1])
    returned = lax.all_to_all(result, "ep", split_axis=0, concat_axis=0, tiled=True)
    mixer_output = mixer_total.astype(jnp.bfloat16)
    results = returned.reshape(experts * capacity, returned.shape[2])
    picked = results[target].astype(jnp.float32).reshape(rows_here, TOP_K, returned.shape[2])
    expert_output = jnp.sum(picked * chances[:, :, None], axis=1).astype(jnp.bfloat16)
    return (mixer_output, expert_output)


def solution(mesh):
    return jax.shard_map(
        shards,
        mesh=mesh,
        in_specs=(
            P("ep", None),
            P(),
            P(None, "tp"),
            P(None, "tp"),
            P(None, "tp"),
            P(None, "tp"),
            P("tp"),
            P("ep", None),
            P(),
            P("ep", None),
            P("ep", None),
            P("ep", None, "tp"),
            P("ep", None, "tp"),
            P("ep", None, "tp"),
        ),
        out_specs=(P("ep", "tp"), P("ep", "tp")),
        check_vma=False,
    )
```

profile of v0, /device:TPU:0, one launch (start us, length us, event | category | flops | bytes accessed | tf_op | source)
XLA Modules:
  0.0 214.6 jit_solution(16968832232059653629)
XLA Ops:
  9.1 1.2 fusion.19
  10.3 1.1 reduce-window.6
  12.0 2.4 %scatter_custom_fusion = s32[1024]{0:T(1024)S(1)} fusion(s32[512]{0:T(512)S(1)} %bitcast.98, s32[512]{0:T(512)S(1)} %add_select_fusion, s32[]{:T(128)} %constant.101.clone.1), kind=kCustom, calls=%fused_computation.95 | custom fusion | bytes 4100 | tf_op jit(solution)/shard_map/scatter | solution.py:147
  14.5 1.2 fusion.21
  15.8 4.0 %gather_fusion = bf16[1024,512]{1,0:T(8,128)(2,1)S(1)} fusion(bf16[129,512]{1,0:T(8,128)(2,1)S(1)} %pad_dynamic-slice_fusion, s32[1024]{0:T(1024)S(1)} %fusion.37), kind=kCustom, calls=%fused_computation | custom fusion | bytes 2101248 | tf_op jit(solution)/shard_map/gather | solution.py:157
  19.7 32.8 %all_to_all.10 = bf16[8,128,512]{2,1,0:T(8,128)(2,1)} all-to-all(bf16[8,128,512]{2,1,0:T(8,128)(2,1)S(1)} %bitcast.89), channel_id=1, replica_groups=mesh['ep'=8,'tp'=4] {'ep'}, dimensions={0} | all-to-all | bytes 2097152 | tf_op jit(solution)/shard_map/all_to_all | solution.py:158
  52.6 51.5 %all-gather.6.cloned.1.call-done = bf16[1024,2048]{1,0:T(8,128)(2,1)} async-done(((bf16[1024,512]{1,0:T(8,128)(2,1)}), bf16[1024,2048]{1,0:T(8,128)(2,1)}) %all-gather.6.cloned.1.call-update) | async-done | bytes 4194320 | tf_op jit(solution)/shard_map/all_gather | solution.py:161
  104.1 4.7 %fusion.7 = f32[1024,512]{1,0:T(8,128)S(1)} fusion(bf16[1024,2048]{1,0:T(8,128)(2,1)} %all-gather.6.cloned.1.call-done, bf16[1,2048,512]{2,1,0:T(8,128)(2,1)S(1)} %copy-done), kind=kOutput, calls=%fused_computation.15 | convolution fusion | flops 2147483648 | bytes 8388608 | tf_op jit(solution)/shard_map/dot_general | solution.py:66
  108.8 3.8 %multiply_convert_fusion = bf16[1024,512]{1,0:T(8,128)(2,1)} fusion(f32[1024,512]{1,0:T(8,128)S(1)} %fusion.7, bf16[1024,2048]{1,0:T(8,128)(2,1)S(1)} %copy-done.4, bf16[1,2048,512]{2,1,0:T(8,128)(2,1)S(1)} %copy-done.5), kind=kOutput, calls=%fused_computation.19 | convolution fusion | flops 2152726528 | bytes 9437184 | tf_op jit(solution)/shard_map/dot_general | solution.py:66
  113.4 1.9 fusion.56
  116.8 2.2 %collective-permute-start = (bf16[128,512]{0,1:T(8,128)(2,1)}, bf16[128,512]{0,1:T(8,128)(2,1)}, u32[]{:S(2)}, u32[]{:S(2)}) collective-permute-start(bf16[128,512]{0,1:T(8,128)(2,1)} %get-tuple-element.16), channel_id=1, source_target_pairs={{0,4},{4,8},{8,12},{12,16},{16,20},{20,24},{24,28},{1,5},{5,9},{9,... | collective-permute-start | bytes 393224 | tf_op jit(solution)/shard_map/ppermute | solution.py:23
  119.0 1.6 collective-permute-start.1
  120.6 1.1 fusion.53
  125.1 1.0 pad_maximum_fusion.1
  126.6 1.6 fusion.1
  131.1 34.2 %all-gather.8.cloned.1.call-done = bf16[1024,2048]{1,0:T(8,128)(2,1)} async-done(((bf16[1024,512]{1,0:T(8,128)(2,1)}), bf16[1024,2048]{1,0:T(8,128)(2,1)}) %all-gather.8.cloned.1.call-update) | async-done | bytes 4194320 | tf_op jit(solution)/shard_map/all_gather | solution.py:166
  165.3 6.2 %fusion.14 = bf16[1024,512]{1,0:T(8,128)(2,1)} fusion(bf16[1024,2048]{1,0:T(8,128)(2,1)} %all-gather.8.cloned.1.call-done, bf16[1,2048,512]{2,1,0:T(8,128)(2,1)} %param.27), kind=kOutput, calls=%fused_computation.21 | convolution fusion | flops 2148007936 | bytes 7340032 | tf_op jit(solution)/shard_map/dot_general | solution.py:66
  171.5 4.7 %all-to-all-start.1 = ((bf16[8,128,512]{2,1,0:T(8,128)(2,1)}), bf16[8,128,512]{2,1,0:T(8,128)(2,1)S(1)}, u32[]{:S(2)}, u32[]{:S(2)}) async-start(bf16[8,128,512]{2,1,0:T(8,128)(2,1)} %bitcast.93), calls=%async_computation.1 | async-start | bytes 2097152 | tf_op jit(solution)/shard_map/all_to_all | solution.py:168
  176.4 17.9 %all-gather.4.cloned.1.call-done = bf16[256,2048]{0,1:T(8,128)(2,1)} async-done(((bf16[256,512]{0,1:T(8,128)(2,1)}), bf16[256,2048]{0,1:T(8,128)(2,1)}) %all-gather.4.cloned.1.call-update) | async-done | bytes 1048592 | tf_op jit(solution)/shard_map/all_gather | solution.py:160
  194.2 3.3 %convolution_convert_fusion = bf16[256,512]{1,0:T(8,128)(2,1)} fusion(bf16[256,2048]{0,1:T(8,128)(2,1)} %all-gather.4.cloned.1.call-done, bf16[2048,512]{1,0:T(8,128)(2,1)} %param.19), kind=kOutput, calls=%fused_computation.24 | convolution fusion | flops 537001984 | bytes 3407872 | tf_op jit(solution)/shard_map/dot_general | solution.py:66
  197.6 5.2 %all-to-all-done.1 = bf16[8,128,512]{2,1,0:T(8,128)(2,1)S(1)} async-done(((bf16[8,128,512]{2,1,0:T(8,128)(2,1)}), bf16[8,128,512]{2,1,0:T(8,128)(2,1)S(1)}, u32[]{:S(2)}, u32[]{:S(2)}) %all-to-all-start.1) | async-done | bytes 1048608 | tf_op jit(solution)/shard_map/all_to_all | solution.py:168
  202.8 2.6 %gather_fusion.1 = bf16[512,512]{1,0:T(8,128)(2,1)} fusion(bf16[1024,512]{1,0:T(8,128)(2,1)S(1)} %bitcast.88, s32[1024]{0:T(1024)S(1)} %pad_clamp_fusion), kind=kCustom, calls=%fused_computation.1 | custom fusion | bytes 1050624 | tf_op jit(solution)/shard_map/gather | solution.py:171
  205.4 1.4 reshape.338
  206.7 1.4 multiply_reduce_fusion
  (83 shorter events, 11.5 us)
Async XLA Ops:
  7.2 97.0 %copy-start = (bf16[1,2048,512]{2,1,0:T(8,128)(2,1)S(1)}, bf16[1,2048,512]{2,1,0:T(8,128)(2,1)}, u32[]{:S(2)}) copy-start(bf16[1,2048,512]{2,1,0:T(8,128)(2,1)} %param.26) | copy-start | bytes 6291460
  7.2 96.9 %all-gather.6.cloned.1.call-start = ((), (), s32[]{:S(2)}) async-start(), calls=%async_computation.3 | async-start | bytes 5242880 | tf_op jit(solution)/shard_map/all_gather | solution.py:161
  52.6 112.7 %all-gather.8.cloned.1.call-start = ((), (), s32[]{:S(2)}) async-start(), calls=%async_computation.4 | async-start | bytes 5242880 | tf_op jit(solution)/shard_map/all_gather | solution.py:166
  104.1 4.7 %copy-start.4 = (bf16[1024,2048]{1,0:T(8,128)(2,1)S(1)}, bf16[1024,2048]{1,0:T(8,128)(2,1)}, u32[]{:S(2)}) copy-start(bf16[1024,2048]{1,0:T(8,128)(2,1)} %all-gather.6.cloned.1.call-done) | copy-start | bytes 12582916
  104.1 4.7 %copy-start.5 = (bf16[1,2048,512]{2,1,0:T(8,128)(2,1)S(1)}, bf16[1,2048,512]{2,1,0:T(8,128)(2,1)}, u32[]{:S(2)}) copy-start(bf16[1,2048,512]{2,1,0:T(8,128)(2,1)} %param.25) | copy-start | bytes 6291460
  108.8 4.0 %copy-start.1 = (bf16[256,2048]{1,0:T(8,128)(2,1)S(1)}, bf16[256,2048]{1,0:T(8,128)(2,1)}, u32[]{:S(2)}) copy-start(bf16[256,2048]{1,0:T(8,128)(2,1)} %param.14) | copy-start | bytes 3145732
  112.7 0.7 copy-start.8
  112.7 81.5 %all-gather.4.cloned.1.call-start = ((), (), s32[]{:S(2)}) async-start(), calls=%async_computation.2 | async-start | bytes 1310720 | tf_op jit(solution)/shard_map/all_gather | solution.py:160
  113.1 2.3 %copy-start.7 = (bf16[2048,256]{1,0:T(8,128)(2,1)S(1)}, bf16[2048,256]{1,0:T(8,128)(2,1)}, u32[]{:S(2)}) copy-start(bf16[2048,256]{1,0:T(8,128)(2,1)} %param.18) | copy-start | bytes 3145732
  115.3 5.3 %copy-start.6 = (bf16[2048,512]{1,0:T(8,128)(2,1)S(1)}, bf16[2048,512]{1,0:T(8,128)(2,1)}, u32[]{:S(2)}) copy-start(bf16[2048,512]{1,0:T(8,128)(2,1)} %param.16) | copy-start | bytes 6291460
  116.8 8.3 %collective-permute-start = (bf16[128,512]{0,1:T(8,128)(2,1)}, bf16[128,512]{0,1:T(8,128)(2,1)}, u32[]{:S(2)}, u32[]{:S(2)}) collective-permute-start(bf16[128,512]{0,1:T(8,128)(2,1)} %get-tuple-element.16), channel_id=1, source_target_pairs={{0,4},{4,8},{8,12},{12,16},{16,20},{20,24},{24,28},{1,5},{5,9},{9,... | collective-permute-start | bytes 393224 | tf_op jit(solution)/shard_map/ppermute | solution.py:23
  119.0 5.4 %copy-start.3 = (f32[8]{0:T(128)S(1)}, f32[8]{0:T(128)}, u32[]{:S(2)}) copy-start(f32[8]{0:T(128)} %param.20) | copy-start | bytes 100
  119.0 6.1 %collective-permute-start.1 = (bf16[128,512]{0,1:T(8,128)(2,1)}, bf16[128,512]{0,1:T(8,128)(2,1)}, u32[]{:S(2)}, u32[]{:S(2)}) collective-permute-start(bf16[128,512]{0,1:T(8,128)(2,1)} %get-tuple-element.15), channel_id=1, source_target_pairs={{4,0},{8,4},{12,8},{16,12},{20,16},{24,20},{28,24},{5,1},{9,5},{13... | collective-permute-start | bytes 393224 | tf_op jit(solution)/shard_map/ppermute | solution.py:24
  171.5 4.7 %copy-start.2 = (f32[128,4]{0,1:T(4,128)S(1)}, f32[128,4]{0,1:T(4,128)}, u32[]{:S(2)}) copy-start(f32[128,4]{0,1:T(4,128)} %param.24) | copy-start | bytes 6148
  171.5 31.3 %all-to-all-start.1 = ((bf16[8,128,512]{2,1,0:T(8,128)(2,1)}), bf16[8,128,512]{2,1,0:T(8,128)(2,1)S(1)}, u32[]{:S(2)}, u32[]{:S(2)}) async-start(bf16[8,128,512]{2,1,0:T(8,128)(2,1)} %bitcast.93), calls=%async_computation.1 | async-start | bytes 2097152 | tf_op jit(solution)/shard_map/all_to_all | solution.py:168
Sparse Core Ops, SparseCore 0:
  52.7 51.3 all-gather.5
  112.8 52.4 all-gather.7
  167.7 26.4 all-gather.3
where the time goes:
time: 215 us
  waiting for transfers between devices  109 us (51%)
  blocking collectives  32.8 us (15%)
  matrix products  24.2 us (11%)
  local copies, waits for them, and re-layouts  16.3 us (8%)
  between operations  14.1 us (7%)
  other arithmetic  9.73 us (5%)
  starting transfers between devices  8.66 us (4%)
    all_gather x1, waiting for transfers between devices, shards(): feature_piece = lax.all_gather(flat, 'tp', axis=1, tiled=True)  51.5 us
    all_gather x1, waiting for transfers between devices, shards(): lax.all_gather(hidden, 'tp', axis=1, tiled=True)  34.2 us
    all_to_all x1, blocking collectives, shards(): lax.all_to_all(outgoing, 'ep', split_axis=0, concat_axis=0, tiled=True)  32.8 us
    dot_general x4, matrix products, add_product(): return jnp.dot(piece, weight, preferred_element_type=jnp.float32)  18 us
    all_gather x1, waiting for transfers between devices, shards(): head_piece = lax.all_gather(mixed, 'tp', axis=1, tiled=True)  17.9 us
    all_to_all x1, waiting for transfers between devices, shards(): lax.all_to_all(result, 'ep', split_axis=0, concat_axis=0, tiled=True)  5.17 us
    all_to_all x1, starting transfers between devices, shards(): lax.all_to_all(result, 'ep', split_axis=0, concat_axis=0, tiled=True)  4.74 us
  transfers between devices with their start and end apart: 6, of which 4 were waited for; matrix products, arithmetic and copies ran while one was open for 11% of the time, Pallas kernels for 0%

commit v1 on v0

--- a/solution.py
+++ b/solution.py
@@ -158,7 +158,15 @@
     received = lax.all_to_all(outgoing, "ep", split_axis=0, concat_axis=0, tiled=True)
     flat = received.reshape(experts * capacity, width)
     head_piece = lax.all_gather(mixed, "tp", axis=1, tiled=True)
-    feature_piece = lax.all_gather(flat, "tp", axis=1, tiled=True)
+    how_many = lax.axis_size("tp")
+    lower = [None] * how_many
+    table = [(hop_no, (hop_no + 1) % how_many) for hop_no in range(how_many)]
+    lower[how_many - 1] = flat
+    for s in range(how_many - 2, -1, -1):
+        lower[s] = lax.ppermute(lower[s + 1], axis_name="tp", perm=table)
+    block_next = jnp.concatenate(lower, axis=1)
+    h_now = lax.axis_index("tp")
+    feature_piece = jnp.roll(block_next, (h_now + 1) * flat.shape[1], axis=1)
     mixer_total = add_product(head_piece, output_weight)
     gate = add_product(feature_piece, gate_local)
     up = add_product(feature_piece, up_local)

time: 215 us -> 244 us (1.13)
  waiting for transfers between devices: 109 us -> 130 us
  local copies, waits for them, and re-layouts: 16.3 us -> 25 us
  matrix products: 24.2 us -> 21 us
    ppermute x0 -> x3, waiting for transfers between devices: none -> 72.1 us  [shards(): lower[s] = lax.ppermute(lower[s + 1], axis_name='tp', perm=table)]
    all_gather x1 -> x0, waiting for transfers between devices: 51.5 us -> none  [shards(): feature_piece = lax.all_gather(flat, 'tp', axis=1, tiled=True)]
    unnamed x22 -> x39, local copies, waits for them, and re-layouts: 1.9 us -> 9.3 us
  transfers between devices with their start and end apart: 6 -> 8, of which waited for: 4 -> 6; matrix products, arithmetic and copies ran while one was open for 11% -> 10% of each run, Pallas kernels for 0% -> 0%
where the time goes in v1:
time: 244 us; the launch traced here: 243 us
  waiting for transfers between devices  130 us (53%)
  blocking collectives  32.9 us (13%)
  local copies, waits for them, and re-layouts  25 us (10%)
  matrix products  21 us (9%)
  between operations  14.5 us (6%)
  starting transfers between devices  10.3 us (4%)
  other arithmetic  9.73 us (4%)
    ppermute x3, waiting for transfers between devices, shards(): lower[s] = lax.ppermute(lower[s + 1], axis_name='tp', perm=table)  72.1 us
    all_gather x1, waiting for transfers between devices, shards(): lax.all_gather(hidden, 'tp', axis=1, tiled=True)  34.6 us
    all_to_all x1, blocking collectives, shards(): lax.all_to_all(outgoing, 'ep', split_axis=0, concat_axis=0, tiled=True)  32.9 us
    all_gather x1, waiting for transfers between devices, shards(): head_piece = lax.all_gather(mixed, 'tp', axis=1, tiled=True)  18 us
    dot_general x4, matrix products, add_product(): return jnp.dot(piece, weight, preferred_element_type=jnp.float32)  15.6 us
    unnamed x39, local copies, waits for them, and re-layouts  9.3 us
    gather x1, local copies, waits for them, and re-layouts, shards(): outgoing = own[source].reshape(experts, capacity, width)  5.08 us
    all_to_all x1, waiting for transfers between devices, shards(): lax.all_to_all(result, 'ep', split_axis=0, concat_axis=0, tiled=True)  5.04 us
  transfers between devices with their start and end apart: 8, of which 6 were waited for; matrix products, arithmetic and copies ran while one was open for 10% of the time, Pallas kernels for 0%

profile of v1, /device:TPU:0, one launch (start us, length us, event | category | flops | bytes accessed | tf_op | source)
XLA Modules:
  0.0 243.2 jit_solution(11483940394623511079)
XLA Ops:
  12.0 2.4 %scatter_custom_fusion = s32[1024]{0:T(1024)S(1)} fusion(s32[512]{0:T(512)S(1)} %bitcast.98, s32[512]{0:T(512)S(1)} %add_select_fusion, s32[]{:T(128)} %constant.120.clone.1), kind=kCustom, calls=%fused_computation.105 | custom fusion | bytes 4100 | tf_op jit(solution)/shard_map/scatter | solution.py:147
  15.8 5.1 %gather_fusion = bf16[1024,512]{1,0:T(8,128)(2,1)} fusion(bf16[129,512]{1,0:T(8,128)(2,1)S(1)} %pad_dynamic-slice_fusion, s32[1024]{0:T(1024)S(1)} %fusion.41), kind=kCustom, calls=%fused_computation | custom fusion | bytes 2101248 | tf_op jit(solution)/shard_map/gather | solution.py:157
  20.9 32.9 %all_to_all.10 = bf16[8,128,512]{2,1,0:T(8,128)(2,1)S(1)} all-to-all(bf16[8,128,512]{2,1,0:T(8,128)(2,1)} %bitcast.90), channel_id=1, replica_groups=mesh['ep'=8,'tp'=4] {'ep'}, dimensions={0} | all-to-all | bytes 2097152 | tf_op jit(solution)/shard_map/all_to_all | solution.py:158
  53.8 1.5 collective-permute-start.2
  55.3 23.9 %collective-permute-done.2 = bf16[1024,512]{1,0:T(8,128)(2,1)S(1)} collective-permute-done((bf16[1024,512]{1,0:T(8,128)(2,1)S(1)}, bf16[1024,512]{1,0:T(8,128)(2,1)S(1)}, u32[]{:S(2)}, u32[]{:S(2)}) %collective-permute-start.2) | collective-permute-done | bytes 1048608 | tf_op jit(solution)/shard_map/ppermute | solution.py:166
  80.8 24.1 %collective-permute-done.3 = bf16[1024,512]{1,0:T(8,128)(2,1)} collective-permute-done((bf16[1024,512]{1,0:T(8,128)(2,1)S(1)}, bf16[1024,512]{1,0:T(8,128)(2,1)}, u32[]{:S(2)}, u32[]{:S(2)}) %collective-permute-start.3) | collective-permute-done | bytes 1048608 | tf_op jit(solution)/shard_map/ppermute | solution.py:166
  104.9 24.0 %collective-permute-done.4 = bf16[1024,512]{1,0:T(8,128)(2,1)} collective-permute-done((bf16[1024,512]{1,0:T(8,128)(2,1)}, bf16[1024,512]{1,0:T(8,128)(2,1)}, u32[]{:S(2)}, u32[]{:S(2)}) %collective-permute-start.4) | collective-permute-done | bytes 1048608 | tf_op jit(solution)/shard_map/ppermute | solution.py:166
  128.9 1.4 constant_dynamic-update-slice_fusion.7
  130.3 1.4 constant_dynamic-update-slice_fusion.6
  132.0 1.4 constant_dynamic-update-slice_fusion.3
  133.4 1.4 constant_dynamic-update-slice_fusion.2
  135.2 2.3 fusion.2
  137.5 3.8 %multiply_convert_fusion = bf16[1024,512]{1,0:T(8,128)(2,1)} fusion(f32[1024,512]{1,0:T(8,128)S(1)} %fusion.2, bf16[1,2048,512]{2,1,0:T(8,128)(2,1)S(1)} %copy-done.10, bf16[1024,4096]{1,0:T(8,128)(2,1)S(1)} %constant_dynamic-update-slice_fusion, s32[]{:T(128)S(6)} %select_n.69), kind=kOutput, calls=%fused_computation.21 | convolution fusion | flops 2152726528 | bytes 9437188 | tf_op jit(solution)/shard_map/dot_general | solution.py:66
  141.9 2.0 fusion.62
  145.5 2.1 collective-permute-start
  147.5 1.5 collective-permute-start.1
  159.1 34.6 %all-gather.5.cloned.1.call-done = bf16[1024,2048]{1,0:T(8,128)(2,1)} async-done(((bf16[1024,512]{1,0:T(8,128)(2,1)}), bf16[1024,2048]{1,0:T(8,128)(2,1)}) %all-gather.5.cloned.1.call-update) | async-done | bytes 4194320 | tf_op jit(solution)/shard_map/all_gather | solution.py:174
  193.7 6.2 %fusion.18 = bf16[1024,512]{1,0:T(8,128)(2,1)} fusion(bf16[1024,2048]{1,0:T(8,128)(2,1)} %all-gather.5.cloned.1.call-done, bf16[1,2048,512]{2,1,0:T(8,128)(2,1)} %param.27), kind=kOutput, calls=%fused_computation.23 | convolution fusion | flops 2148007936 | bytes 7340032 | tf_op jit(solution)/shard_map/dot_general | solution.py:66
  199.8 4.6 %all-to-all-start.1 = ((bf16[8,128,512]{2,1,0:T(8,128)(2,1)}), bf16[8,128,512]{2,1,0:T(8,128)(2,1)S(1)}, u32[]{:S(2)}, u32[]{:S(2)}) async-start(bf16[8,128,512]{2,1,0:T(8,128)(2,1)} %bitcast.93), calls=%async_computation.1 | async-start | bytes 2097152 | tf_op jit(solution)/shard_map/all_to_all | solution.py:176
  204.6 18.0 %all-gather.3.cloned.1.call-done = bf16[256,2048]{0,1:T(8,128)(2,1)} async-done(((bf16[256,512]{0,1:T(8,128)(2,1)}), bf16[256,2048]{0,1:T(8,128)(2,1)}) %all-gather.3.cloned.1.call-update) | async-done | bytes 1048592 | tf_op jit(solution)/shard_map/all_gather | solution.py:160
  222.6 3.3 %convolution_convert_fusion = bf16[256,512]{1,0:T(8,128)(2,1)} fusion(bf16[256,2048]{0,1:T(8,128)(2,1)} %all-gather.3.cloned.1.call-done, bf16[2048,512]{1,0:T(8,128)(2,1)} %param.19), kind=kOutput, calls=%fused_computation.26 | convolution fusion | flops 537001984 | bytes 3407872 | tf_op jit(solution)/shard_map/dot_general | solution.py:66
  226.0 5.0 %all-to-all-done.1 = bf16[8,128,512]{2,1,0:T(8,128)(2,1)S(1)} async-done(((bf16[8,128,512]{2,1,0:T(8,128)(2,1)}), bf16[8,128,512]{2,1,0:T(8,128)(2,1)S(1)}, u32[]{:S(2)}, u32[]{:S(2)}) %all-to-all-start.1) | async-done | bytes 1048608 | tf_op jit(solution)/shard_map/all_to_all | solution.py:176
  231.0 2.6 %gather_fusion.1 = bf16[512,512]{1,0:T(8,128)(2,1)} fusion(bf16[1024,512]{1,0:T(8,128)(2,1)S(1)} %bitcast.86, s32[1024]{0:T(1024)S(1)} %pad_clamp_fusion), kind=kCustom, calls=%fused_computation.1 | custom fusion | bytes 1050624 | tf_op jit(solution)/shard_map/gather | solution.py:179
  233.6 1.4 reshape.338
  (104 shorter events, 21.9 us)
Async XLA Ops:
  7.2 128.0 %copy-start = (bf16[1,2048,512]{2,1,0:T(8,128)(2,1)S(1)}, bf16[1,2048,512]{2,1,0:T(8,128)(2,1)}, u32[]{:S(2)}) copy-start(bf16[1,2048,512]{2,1,0:T(8,128)(2,1)} %param.25) | copy-start | bytes 6291460
  7.2 186.5 %all-gather.5.cloned.1.call-start = ((), (), s32[]{:S(2)}) async-start(), calls=%async_computation.3 | async-start | bytes 5242880 | tf_op jit(solution)/shard_map/all_gather | solution.py:174
  53.8 25.4 %collective-permute-start.2 = (bf16[1024,512]{1,0:T(8,128)(2,1)S(1)}, bf16[1024,512]{1,0:T(8,128)(2,1)S(1)}, u32[]{:S(2)}, u32[]{:S(2)}) collective-permute-start(bf16[1024,512]{1,0:T(8,128)(2,1)S(1)} %bitcast.87), channel_id=1, source_target_pairs={{0,1},{1,2},{2,3},{3,0},{4,5},{5,6},{6,7},{7,4},{8,9},{9,10},{10,1... | collective-permute-start | bytes 3145736 | tf_op jit(solution)/shard_map/ppermute | solution.py:166
  79.2 1.0 copy-start.1
  80.2 24.7 %collective-permute-start.3 = (bf16[1024,512]{1,0:T(8,128)(2,1)S(1)}, bf16[1024,512]{1,0:T(8,128)(2,1)}, u32[]{:S(2)}, u32[]{:S(2)}) collective-permute-start(bf16[1024,512]{1,0:T(8,128)(2,1)S(1)} %collective-permute-done.2), channel_id=1, source_target_pairs={{0,1},{1,2},{2,3},{3,0},{4,5},{5,6},{6,7},{7,4},{8,9},{9,10},{10,1... | collective-permute-start | bytes 3145736 | tf_op jit(solution)/shard_map/ppermute | solution.py:166
  104.9 24.0 %collective-permute-start.4 = (bf16[1024,512]{1,0:T(8,128)(2,1)}, bf16[1024,512]{1,0:T(8,128)(2,1)}, u32[]{:S(2)}, u32[]{:S(2)}) collective-permute-start(bf16[1024,512]{1,0:T(8,128)(2,1)} %collective-permute-done.3), channel_id=1, source_target_pairs={{0,1},{1,2},{2,3},{3,0},{4,5},{5,6},{6,7},{7,4},{8,9},{9,10},{10,1... | collective-permute-start | bytes 3145736 | tf_op jit(solution)/shard_map/ppermute | solution.py:166
  104.9 26.8 %copy-start.2 = (bf16[1024,512]{1,0:T(8,128)(2,1)S(1)}, bf16[1024,512]{1,0:T(8,128)(2,1)}, u32[]{:S(2)}) copy-start(bf16[1024,512]{1,0:T(8,128)(2,1)} %copy-done.1) | copy-start | bytes 3145732
  135.1 2.3 copy-start.10
  137.5 3.9 %copy-start.3 = (bf16[256,2048]{1,0:T(8,128)(2,1)S(1)}, bf16[256,2048]{1,0:T(8,128)(2,1)}, u32[]{:S(2)}) copy-start(bf16[256,2048]{1,0:T(8,128)(2,1)} %param.14) | copy-start | bytes 3145732
  137.5 4.4 %copy-start.13 = (f32[2048]{0:T(1024)S(1)}, f32[2048]{0:T(1024)}, u32[]{:S(2)}) copy-start(f32[2048]{0:T(1024)} %param.15) | copy-start | bytes 24580
  141.3 81.3 %all-gather.3.cloned.1.call-start = ((), (), s32[]{:S(2)}) async-start(), calls=%async_computation.2 | async-start | bytes 1310720 | tf_op jit(solution)/shard_map/all_gather | solution.py:160
  141.4 2.7 %copy-start.12 = (bf16[2048,256]{1,0:T(8,128)(2,1)S(1)}, bf16[2048,256]{1,0:T(8,128)(2,1)}, u32[]{:S(2)}) copy-start(bf16[2048,256]{1,0:T(8,128)(2,1)} %param.18) | copy-start | bytes 3145732
  141.9 7.1 %copy-start.11 = (bf16[2048,512]{1,0:T(8,128)(2,1)S(1)}, bf16[2048,512]{1,0:T(8,128)(2,1)}, u32[]{:S(2)}) copy-start(bf16[2048,512]{1,0:T(8,128)(2,1)} %param.16) | copy-start | bytes 6291460
  145.5 7.4 %copy-start.9 = (f32[8]{0:T(128)S(1)}, f32[8]{0:T(128)}, u32[]{:S(2)}) copy-start(f32[8]{0:T(128)} %param.20) | copy-start | bytes 100
  145.5 8.1 %collective-permute-start = (bf16[128,512]{0,1:T(8,128)(2,1)}, bf16[128,512]{0,1:T(8,128)(2,1)}, u32[]{:S(2)}, u32[]{:S(2)}) collective-permute-start(bf16[128,512]{0,1:T(8,128)(2,1)} %get-tuple-element.16), channel_id=1, source_target_pairs={{0,4},{4,8},{8,12},{12,16},{16,20},{20,24},{24,28},{1,5},{5,9},{9,... | collective-permute-start | bytes 393224 | tf_op jit(solution)/shard_map/ppermute | solution.py:23
  147.5 6.0 %collective-permute-start.1 = (bf16[128,512]{0,1:T(8,128)(2,1)}, bf16[128,512]{0,1:T(8,128)(2,1)}, u32[]{:S(2)}, u32[]{:S(2)}) collective-permute-start(bf16[128,512]{0,1:T(8,128)(2,1)} %get-tuple-element.15), channel_id=1, source_target_pairs={{4,0},{8,4},{12,8},{16,12},{20,16},{24,20},{28,24},{5,1},{9,5},{13... | collective-permute-start | bytes 393224 | tf_op jit(solution)/shard_map/ppermute | solution.py:24
  154.6 0.8 copy-start.4
  154.6 0.9 copy-start.5
  154.6 0.9 copy-start.6
  154.7 0.9 copy-start.7
  159.1 45.4 %copy-start.8 = (f32[128,4]{0,1:T(4,128)S(1)}, f32[128,4]{0,1:T(4,128)}, u32[]{:S(2)}) copy-start(f32[128,4]{0,1:T(4,128)} %param.24) | copy-start | bytes 6148
  199.8 31.2 %all-to-all-start.1 = ((bf16[8,128,512]{2,1,0:T(8,128)(2,1)}), bf16[8,128,512]{2,1,0:T(8,128)(2,1)S(1)}, u32[]{:S(2)}, u32[]{:S(2)}) async-start(bf16[8,128,512]{2,1,0:T(8,128)(2,1)} %bitcast.93), calls=%async_computation.1 | async-start | bytes 2097152 | tf_op jit(solution)/shard_map/all_to_all | solution.py:176
Sparse Core Ops, SparseCore 0:
  141.4 52.2 all-gather.4
  196.1 26.4 all-gather.2
